TPU v7x, 512 devices: a whole 4x4x16 slice. The times are simulated.
512 devices in a mesh: fs: 64 (over z, y), tp: 8 (over x, core).
Axes of the slice: x: 4, y: 4, z: 16, core: 2. Of those that a mesh axis runs over, the one named last changes fastest.
Arguments:
- tokens: bfloat16 [16384, 2048], P('fs', 'tp'), may hold values from -16 to 16, as said below
- mix_gain: bfloat16 [2048], P('tp'), may hold values from 0.099609375 to 1.8984375
- query_weight: bfloat16 [2048, 512], P('fs', 'tp'), may hold values from -0.125 to 0.125
- key_weight: bfloat16 [2048, 512], P('fs', 'tp'), may hold values from -0.125 to 0.125
- value_weight: bfloat16 [2048, 1024], P('fs', 'tp'), may hold values from -0.125 to 0.125
- output_gate_weight: bfloat16 [2048, 1024], P('fs', 'tp'), may hold values from -0.125 to 0.125
- out_weight: bfloat16 [1024, 2048], P('tp', 'fs'), may hold values from -0.1875 to 0.1875
- head_rates: float32 [8], P('tp'), may hold values from 0 to 1, as said below
- block_scale: float32 [128], P('fs'), may hold values from 0.5 to 2
- ffn_gain: bfloat16 [2048], P('tp'), may hold values from 0.099609375 to 1.8984375
- ff_gate: bfloat16 [2048, 5632], P('fs', 'tp'), may hold values from -0.125 to 0.125
- ff_up: bfloat16 [2048, 5632], P('fs', 'tp'), may hold values from -0.125 to 0.125
- ff_down: bfloat16 [5632, 2048], P('tp', 'fs'), may hold values from -0.078125 to 0.078125
- final_gain: bfloat16 [2048], P('tp'), may hold values from 0.099609375 to 1.8984375
Outputs:
- layer_out: bfloat16 [16384, 2048], P('fs', 'tp')
Inputs may be any that keep to these rules, and one draw needn't show every extreme that they name: `tokens`: column blocks of the activations have different scales. `head_rates`: positive rates.
All inputs are finite; a program needn't handle non-finite values.
Results may differ from a plain program's by a relative error of at most 0.014.
Values may be sent and summed in bfloat16 or wider, within the bound.
A program may use at most 64 MiB of HBM per device.

v0:
```python
import jax
import jax.numpy as jnp
from jax import lax
from jax.sharding import Mesh
from jax.sharding import PartitionSpec as P

D = 2048
DK = 64
DV = 128
BLK = 128
SEQ_LEN = 256
FS = ("fs_0", "fs_1")
EPS = 1e-06
THETA = 10000.0


def gather_turned(arrays, axis, dims):
    turned = [jnp.moveaxis(a, dim, 0) for a, dim in zip(arrays, dims)]
    both = jnp.concatenate([t.reshape(len(t), -1) for t in turned], axis=1)
    filled, at, outs = (lax.all_gather(both, axis, axis=0, tiled=True), 0, [])
    for t, dim in zip(turned, dims):
        share = filled[:, at : at + t[0].size].reshape(-1, *t.shape[1:])
        outs.append(jnp.moveaxis(share, 0, dim))
        at += t[0].size
    return tuple(outs)


def sent_together(arrays, axis, dim, along):
    widths = [a.shape[along] for a in arrays]
    both = jnp.concatenate(arrays, axis=along)
    filled = lax.all_gather(both, axis, axis=dim, tiled=True)
    return tuple(jnp.split(filled, [sum(widths[:k]) for k in range(1, len(widths))], axis=along))


def laid_out(tiles, dim):
    lengths = list(tiles.shape[1:])
    lengths[dim] *= tiles.shape[0]
    return jnp.moveaxis(tiles, 0, dim).reshape(lengths)


def copy_for_each(shard, axis):
    size = lax.axis_size(axis)
    return lax.all_to_all(
        jnp.broadcast_to(shard[None], (size, *shard.shape)), axis, 0, 0, tiled=True
    )


def gather_directly(shard, axis, dim):
    return laid_out(copy_for_each(shard, axis), dim)


def gathered_by_axis(shard, axes, dim):
    filled = shard
    for number in range(len(axes) - 1, -1, -1):
        filled = lax.all_gather(filled, axes[number], axis=dim, tiled=True)
    return filled


def in_blocks(shard, dim, size):
    lengths = shard.shape
    tiles = shard.reshape(*lengths[:dim], size, lengths[dim] // size, *lengths[dim + 1 :])
    return jnp.moveaxis(tiles, dim, 0)


def sent_and_summed(shard, axis, dim):
    size = lax.axis_size(axis)
    tiles = lax.all_to_all(in_blocks(shard, dim, size), axis, 0, 0, tiled=True)
    return jnp.sum(tiles.astype(jnp.float32), axis=0)


def of_everyone(shard, axis):
    return copy_for_each(shard, axis).sum(axis=0)


def rms_norm(values, gain):
    scale = lax.rsqrt(jnp.mean(values * values, axis=-1, keepdims=True) + EPS)
    return values * scale * gain.astype(jnp.float32)


def rotate(values, positions):
    half = values.shape[-1] // 2
    inverse = THETA ** (-jnp.arange(half, dtype=jnp.float32) / half)
    angle = positions.astype(jnp.float32)[:, None] * inverse
    cosine = jnp.cos(angle)[:, None, :]
    sine = jnp.sin(angle)[:, None, :]
    first = values[..., :half]
    second = values[..., half:]
    return jnp.concatenate(
        [first * cosine - second * sine, second * cosine + first * sine], axis=-1
    )


def retain(query, key, value, rates, scales):
    rows, heads_here, width_k = query.shape
    width_v = value.shape[-1]
    nblk = rows // BLK
    hi = lax.Precision.HIGHEST
    qblk = query.astype(jnp.float32).reshape(nblk, BLK, heads_here, width_k)
    kblk = key.astype(jnp.float32).reshape(nblk, BLK, heads_here, width_k)
    vblk = value.astype(jnp.float32).reshape(nblk, BLK, heads_here, width_v)
    logdec = -rates[None, :] * scales[:, None]
    steps = jnp.arange(BLK, dtype=jnp.float32)
    offset = steps[:, None] - steps[None, :]
    causal = offset >= 0
    inside = jnp.where(
        causal[None, None],
        jnp.exp(logdec[:, :, None, None] * jnp.where(causal, offset, 0.0)[None, None]),
        0.0,
    )
    scores = jnp.einsum("nchd,nmhd->nhcm", qblk, kblk, precision=hi) * inside
    inner = jnp.einsum("nhcm,nmhe->nche", scores, vblk, precision=hi)
    zeta = jnp.exp(logdec[:, :, None] * (BLK - 1.0 - steps)[None, None, :])
    kv_block = jnp.einsum(
        "nchd,nche->nhde", kblk * jnp.transpose(zeta, (0, 2, 1))[..., None], vblk, precision=hi
    )
    hold = jnp.exp(logdec * BLK)
    per_seq = SEQ_LEN // BLK
    fresh = (jnp.arange(nblk, dtype=jnp.int32) % per_seq == 0).astype(jnp.float32)

    def advance(state, inputs):
        kv_now, hold_now, fresh_now = inputs
        before = state * (1.0 - fresh_now)
        return (before * hold_now[:, None, None] + kv_now, before)

    start = jnp.zeros((heads_here, width_k, width_v), jnp.float32)
    _, before = lax.scan(advance, start, (kv_block, hold, fresh))
    xi = jnp.exp(logdec[:, :, None] * (steps + 1.0)[None, None, :])
    cross = jnp.einsum(
        "nchd,nhde->nche", qblk * jnp.transpose(xi, (0, 2, 1))[..., None], before, precision=hi
    )
    total = inner + cross
    total = total * lax.rsqrt(jnp.mean(total * total, axis=-1, keepdims=True) + EPS)
    return total.reshape(rows, heads_here * width_v)


def body(
    tokens,
    mix_gain,
    query_weight,
    key_weight,
    value_weight,
    output_gate_weight,
    out_weight,
    head_rates,
    block_scale,
    ffn_gain,
    ff_gate,
    ff_up,
    ff_down,
    final_gain,
):
    rows = tokens.shape[0]
    heads_here = head_rates.shape[0]
    groups = lax.axis_size("tp")
    positions = jnp.arange(rows, dtype=jnp.int32) % SEQ_LEN
    whole, gain_whole = gather_turned((tokens, mix_gain), "tp", (1, 0))
    normed = rms_norm(whole.astype(jnp.float32), gain_whole).astype(jnp.bfloat16)
    collected = sent_together(
        (query_weight, key_weight, value_weight, output_gate_weight), FS, 0, 1
    )
    qproj, kproj, vproj, gproj = tuple(
        (jnp.dot(normed, weight, preferred_element_type=jnp.float32) for weight in collected)
    )
    query = rotate(qproj.reshape(rows, heads_here, DK), positions).astype(jnp.bfloat16)
    key = (rotate(kproj.reshape(rows, heads_here, DK), positions) * DK ** (-0.5)).astype(
        jnp.bfloat16
    )
    value = vproj.astype(jnp.bfloat16).reshape(rows, heads_here, DV)
    normret = retain(query, key, value, head_rates, block_scale)
    gated = (normret * jax.nn.silu(gproj)).astype(jnp.bfloat16)
    all_heads = gather_directly(gated, "tp", 1)
    head_rows = gathered_by_axis(out_weight, FS, 1)
    feature_block = lax.all_to_all(head_rows, "tp", split_axis=1, concat_axis=0, tiled=True)
    width = all_heads.shape[1] // groups
    left = all_heads.reshape(rows, groups, width)
    right = feature_block.reshape(groups, width, feature_block.shape[1])
    partial_sums = jnp.einsum(
        "rng,nge->nre", left, right, preferred_element_type=jnp.float32
    ).astype(jnp.bfloat16)
    mix = jnp.sum(partial_sums.astype(jnp.float32), axis=0)
    resid = (tokens.astype(jnp.float32) + mix).astype(jnp.bfloat16)
    whole2, gain2 = gather_turned((resid, ffn_gain), "tp", (1, 0))
    normed2 = rms_norm(whole2.astype(jnp.float32), gain2).astype(jnp.bfloat16)
    gate_rows, up_rows = sent_together((ff_gate, ff_up), FS, 0, 1)
    gate_part = jnp.dot(normed2, gate_rows, preferred_element_type=jnp.float32)
    up_part = jnp.dot(normed2, up_rows, preferred_element_type=jnp.float32)
    hidden = (jax.nn.silu(gate_part) * up_part).astype(jnp.bfloat16)
    down_terms = jnp.dot(
        hidden, gathered_by_axis(ff_down, FS, 1), preferred_element_type=jnp.float32
    )
    ffn = sent_and_summed(down_terms.astype(jnp.bfloat16), "tp", 1)
    total = resid.astype(jnp.float32) + ffn
    squares = of_everyone(jnp.sum(total * total, axis=-1, keepdims=True), "tp")
    scale = lax.rsqrt(squares / D + EPS)
    return (total * scale * final_gain.astype(jnp.float32)).astype(jnp.bfloat16)


def solution(mesh):
    finer = Mesh(mesh.devices.reshape(16, 4, mesh.shape["tp"]), ("fs_0", "fs_1", "tp"))
    return jax.shard_map(
        body,
        mesh=finer,
        in_specs=(
            P(FS, "tp"),
            P("tp"),
            P(FS, "tp"),
            P(FS, "tp"),
            P(FS, "tp"),
            P(FS, "tp"),
            P("tp", FS),
            P("tp"),
            P(FS),
            P("tp"),
            P(FS, "tp"),
            P(FS, "tp"),
            P("tp", FS),
            P("tp"),
        ),
        out_specs=P(FS, "tp"),
        check_vma=False,
    )
```

profile of v0, /device:TPU:1, one launch (start us, length us, event | category | flops | bytes accessed | tf_op | source)
XLA Modules:
  0.0 515.7 jit_solution(17452584656318330392)
XLA Ops:
  6.5 0.7 reshape.400
  7.2 1.6 pad_maximum_fusion
  8.8 0.0 all-gather.6.cloned.1.call-update
  8.8 0.0 all-gather.8.cloned.1.call-start
  8.9 1.4 pad_maximum_fusion.3
  10.3 0.0 all-gather.8.cloned.1.call-update
  10.3 10.6 %all_gather.26 = bf16[128,128]{0,1:T(8,128)(2,1)S(1)} all-gather(bf16[128,32]{0,1:T(8,128)(2,1)} %param.22), channel_id=1, replica_groups=mesh['fs_0'=16,'fs_1'=4,'tp'=8] {'fs_1'}, dimensions={1}, use_global_device_ids=true | all-gather | bytes 40960 | tf_op jit(solution)/shard_map/all_gather | solution.py:55
  20.9 31.9 %all_gather.27 = bf16[128,2048]{0,1:T(8,128)(2,1)S(1)} all-gather(bf16[128,128]{0,1:T(8,128)(2,1)S(1)} %all_gather.26), channel_id=1, replica_groups=mesh['fs_0'=16,'fs_1'=4,'tp'=8] {'fs_0'}, dimensions={1}, use_global_device_ids=true | all-gather | bytes 557056 | tf_op jit(solution)/shard_map/all_gather | solution.py:55
  52.8 1.0 copy.31
  53.8 14.1 %all-to-all-start.1 = ((bf16[128,8,256]{2,0,1:T(8,128)(2,1)}), bf16[128,8,256]{2,0,1:T(8,128)(2,1)S(1)}, u32[]{:S(2)}, u32[]{:S(2)}) async-start(bf16[128,8,256]{2,0,1:T(8,128)(2,1)} %copy.31), calls=%async_computation.1 | async-start | bytes 1048576 | tf_op jit(solution)/shard_map/all_to_all | solution.py:173
  68.8 0.1 multiply_exponential_fusion
  68.9 1.6 fusion.4
  70.5 0.8 slice_convert_fusion.1
  71.2 109.0 %all-gather.8.cloned.1.call-done = bf16[2048,384]{1,0:T(8,128)(2,1)} async-done(((bf16[32,384]{1,0:T(8,128)(2,1)}), bf16[2048,384]{1,0:T(8,128)(2,1)}) %all-gather.8.cloned.1.call-update) | async-done | bytes 1572880 | tf_op jit(solution)/shard_map/all_gather | solution.py:31
  180.3 2.0 convolution_bitcast_fusion
  182.3 1.6 convolution_bitcast_fusion.1
  183.9 0.2 fusion.58
  184.2 1.5 convolution_convert_fusion.2
  185.8 0.2 convolution_bitcast_fusion.2
  185.9 5.0 while.13
  185.9 0.6 dynamic_slice.22
  187.2 0.6 constant_dynamic-slice_fusion.2
  187.8 0.7 bitcast_add_fusion.2
  188.5 0.6 dynamic_slice.22
  189.7 0.6 constant_dynamic-slice_fusion.2
  190.3 0.7 bitcast_add_fusion.2
  191.1 0.2 convolution_multiply_fusion
  191.3 0.2 fusion.74
  191.5 0.5 multiply_reduce_fusion.1
  192.0 0.1 broadcast_multiply_fusion
  192.1 0.0 copy-start.7
  192.1 1.6 fusion.35
  193.7 0.0 copy-start.2
  193.7 0.0 copy-start.3
  193.7 0.0 copy-start.4
  193.7 0.0 copy-start.5
  193.7 0.9 broadcast_in_dim.29
  194.6 15.1 %all-to-all-start = ((bf16[8,256,128]{2,1,0:T(8,128)(2,1)}), bf16[8,256,128]{2,1,0:T(8,128)(2,1)S(1)}, u32[]{:S(2)}, u32[]{:S(2)}) async-start(bf16[8,256,128]{2,1,0:T(8,128)(2,1)} %broadcast_in_dim.29), calls=%async_computation | async-start | bytes 1048576 | tf_op jit(solution)/shard_map/all_to_all | solution.py:43
  209.7 9.3 %all-to-all-done = bf16[8,256,128]{2,1,0:T(8,128)(2,1)S(1)} async-done(((bf16[8,256,128]{2,1,0:T(8,128)(2,1)}), bf16[8,256,128]{2,1,0:T(8,128)(2,1)S(1)}, u32[]{:S(2)}, u32[]{:S(2)}) %all-to-all-start) | async-done | bytes 524320 | tf_op jit(solution)/shard_map/all_to_all | solution.py:43
  219.0 0.4 convert_reduce_fusion.1
  219.5 0.7 pad_maximum_fusion.1
  220.2 0.0 all-gather.10.cloned.1.call-update
  220.2 0.0 all-gather.12.cloned.1.call-start
  220.3 0.7 pad_maximum_fusion.2
  221.0 0.0 all-gather.12.cloned.1.call-update
  221.0 0.0 all-gather.14.cloned.1.call-start
  221.1 10.0 %all_gather.30 = bf16[704,128]{0,1:T(8,128)(2,1)} all-gather(bf16[704,32]{0,1:T(8,128)(2,1)S(1)} %copy-done.5), channel_id=1, replica_groups=mesh['fs_0'=16,'fs_1'=4,'tp'=8] {'fs_1'}, dimensions={1}, use_global_device_ids=true | all-gather | bytes 225280 | tf_op jit(solution)/shard_map/all_gather | solution.py:55
  231.0 0.0 all-gather.14.cloned.1.call-update
  231.1 15.0 %all-gather.10.cloned.1.call-done = bf16[2048,257]{0,1:T(8,128)(2,1)} async-done(((bf16[256,257]{0,1:T(8,128)(2,1)}), bf16[2048,257]{0,1:T(8,128)(2,1)}) %all-gather.10.cloned.1.call-update) | async-done | bytes 1052688 | tf_op jit(solution)/shard_map/all_gather | solution.py:20
  246.0 1.5 fusion.7
  247.6 0.8 slice_convert_fusion
  248.3 142.7 %all-gather.12.cloned.1.call-done = bf16[2048,1408]{1,0:T(8,128)(2,1)} async-done(((bf16[32,1408]{1,0:T(8,128)(2,1)}), bf16[2048,1408]{1,0:T(8,128)(2,1)}) %all-gather.12.cloned.1.call-update) | async-done | bytes 5767184 | tf_op jit(solution)/shard_map/all_gather | solution.py:31
  391.0 3.7 fusion.2
  394.7 68.0 %all-gather.14.cloned.1.call-done = bf16[704,2048]{0,1:T(8,128)(2,1)} async-done(((bf16[704,128]{0,1:T(8,128)(2,1)}), bf16[704,2048]{0,1:T(8,128)(2,1)}) %all-gather.14.cloned.1.call-update) | async-done | bytes 2883600 | tf_op jit(solution)/shard_map/all_gather | solution.py:55
  462.7 7.2 %convolution_convert_fusion = bf16[256,2048]{1,0:T(8,128)(2,1)S(1)} fusion(bf16[704,2048]{0,1:T(8,128)(2,1)} %all-gather.14.cloned.1.call-done, bf16[2048,1408]{1,0:T(8,128)(2,1)} %all-gather.12.cloned.1.call-done, f32[256,704]{0,1:T(8,128)S(1)} %fusion.2, f32[2048]{0:T(1024)S(1)} %bitcast.82, f32[256]{0:T(256)S(1)} %add_rsqrt_fusion.1, ...), kind=kOutput, calls=%fused_computation.12 | convolution fusion | flops 1480097792 | bytes 9118720 | tf_op jit(solution)/shard_map/dot_general | solution.py:188
  470.0 0.1 copy.37
  470.0 0.0 copy-start.8
  470.1 28.6 %all_to_all.31 = bf16[8,256,256]{2,1,0:T(8,128)(2,1)S(1)} all-to-all(bf16[8,256,256]{2,1,0:T(8,128)(2,1)S(1)} %bitcast.70), channel_id=1, replica_groups=mesh['fs_0'=16,'fs_1'=4,'tp'=8] {'tp'}, dimensions={0} | all-to-all | bytes 2097152 | tf_op jit(solution)/shard_map/all_to_all | solution.py:67
  498.6 0.1 convert_reduce_fusion
  498.8 0.1 multiply_reduce_fusion
  498.9 0.6 broadcast_in_dim.30
  499.5 4.3 all-to-all-start.3
  503.8 4.6 all-to-all-done.3
  508.4 0.8 multiply_convert_fusion
  (43 shorter events, 0.3 us)
Async XLA Ops:
  6.5 62.2 %copy-start.6 = (f32[2]{0:T(128)S(1)}, f32[2]{0:T(128)}, u32[]{:S(2)}) copy-start(f32[2]{0:T(128)} %param.24) | copy-start | bytes 28
  6.5 62.3 %all-gather.6.cloned.1.call-start = ((), (), s32[]{:S(2)}) async-start(), calls=%async_computation.4 | async-start | bytes 1216512 | tf_op jit(solution)/shard_map/all_gather | solution.py:20
  8.8 171.5 %all-gather.8.cloned.1.call-start = ((), (), s32[]{:S(2)}) async-start(), calls=%async_computation.5 | async-start | bytes 1597440 | tf_op jit(solution)/shard_map/all_gather | solution.py:31
  53.8 139.9 %all-to-all-start.1 = ((bf16[128,8,256]{2,0,1:T(8,128)(2,1)}), bf16[128,8,256]{2,0,1:T(8,128)(2,1)S(1)}, u32[]{:S(2)}, u32[]{:S(2)}) async-start(bf16[128,8,256]{2,0,1:T(8,128)(2,1)} %copy.31), calls=%async_computation.1 | async-start | bytes 1048576 | tf_op jit(solution)/shard_map/all_to_all | solution.py:173
  68.9 113.5 %copy-start = (bf16[2048,257]{0,1:T(8,128)(2,1)S(1)}, bf16[2048,257]{0,1:T(8,128)(2,1)}, u32[]{:S(2)}) copy-start(bf16[2048,257]{0,1:T(8,128)(2,1)} %all-gather.6.cloned.1.call-done) | copy-start | bytes 3158020
  192.1 17.6 %copy-start.7 = (bf16[256]{0:T(256)(128)(2,1)S(1)}, bf16[256]{0:T(256)(128)(2,1)}, u32[]{:S(2)}) copy-start(bf16[256]{0:T(256)(128)(2,1)} %param.25) | copy-start | bytes 1540
  193.7 25.8 %copy-start.2 = (bf16[256,256]{1,0:T(8,128)(2,1)S(1)}, bf16[256,256]{1,0:T(8,128)(2,1)}, u32[]{:S(2)}) copy-start(bf16[256,256]{1,0:T(8,128)(2,1)} %param.16) | copy-start | bytes 393220
  193.7 26.6 %copy-start.3 = (bf16[32,704]{1,0:T(8,128)(2,1)S(1)}, bf16[32,704]{1,0:T(8,128)(2,1)}, u32[]{:S(2)}) copy-start(bf16[32,704]{1,0:T(8,128)(2,1)} %param.27) | copy-start | bytes 135172
  193.7 26.6 %copy-start.4 = (bf16[32,704]{1,0:T(8,128)(2,1)S(1)}, bf16[32,704]{1,0:T(8,128)(2,1)}, u32[]{:S(2)}) copy-start(bf16[32,704]{1,0:T(8,128)(2,1)} %param.26) | copy-start | bytes 135172
  193.7 27.3 %copy-start.5 = (bf16[704,32]{0,1:T(8,128)(2,1)S(1)}, bf16[704,32]{0,1:T(8,128)(2,1)}, u32[]{:S(2)}) copy-start(bf16[704,32]{0,1:T(8,128)(2,1)} %param.28) | copy-start | bytes 135172
  194.6 24.4 %all-to-all-start = ((bf16[8,256,128]{2,1,0:T(8,128)(2,1)}), bf16[8,256,128]{2,1,0:T(8,128)(2,1)S(1)}, u32[]{:S(2)}, u32[]{:S(2)}) async-start(bf16[8,256,128]{2,1,0:T(8,128)(2,1)} %broadcast_in_dim.29), calls=%async_computation | async-start | bytes 1048576 | tf_op jit(solution)/shard_map/all_to_all | solution.py:43
  209.7 36.4 %all-gather.10.cloned.1.call-start = ((), (), s32[]{:S(2)}) async-start(), calls=%async_computation.6 | async-start | bytes 1216512 | tf_op jit(solution)/shard_map/all_gather | solution.py:20
  220.2 170.8 %all-gather.12.cloned.1.call-start = ((), (), s32[]{:S(2)}) async-start(), calls=%async_computation.7 | async-start | bytes 5857280 | tf_op jit(solution)/shard_map/all_gather | solution.py:31
  221.0 241.7 %all-gather.14.cloned.1.call-start = ((), (), s32[]{:S(2)}) async-start(), calls=%async_computation.8 | async-start | bytes 3342336 | tf_op jit(solution)/shard_map/all_gather | solution.py:55
  391.0 71.7 %copy-start.1 = (bf16[2048,257]{0,1:T(8,128)(2,1)S(1)}, bf16[2048,257]{0,1:T(8,128)(2,1)}, u32[]{:S(2)}) copy-start(bf16[2048,257]{0,1:T(8,128)(2,1)} %all-gather.10.cloned.1.call-done) | copy-start | bytes 3158020
  470.0 33.7 %copy-start.8 = (bf16[256]{0:T(256)(128)(2,1)S(1)}, bf16[256]{0:T(256)(128)(2,1)}, u32[]{:S(2)}) copy-start(bf16[256]{0:T(256)(128)(2,1)} %param.29) | copy-start | bytes 1540
  499.5 8.9 %all-to-all-start.3 = ((f32[8,256,1]{1,2,0:T(1,128)}), f32[8,256,1]{1,2,0:T(1,128)S(1)}, u32[]{:S(2)}, u32[]{:S(2)}) async-start(f32[8,256,1]{1,2,0:T(1,128)} %broadcast_in_dim.30), calls=%async_computation.3 | async-start | bytes 16384 | tf_op jit(solution)/shard_map/all_to_all | solution.py:43
Sparse Core Ops, SparseCore 0:
  9.4 36.6 all-gather.5
  49.1 131.1 all-gather.7
  220.3 25.6 all-gather.9
  248.8 142.1 all-gather.11
  392.9 69.7 all-gather.13
where the time goes:
time: 517 us; the launch traced here: 516 us
  waiting for transfers between devices  349 us (68%)
  blocking collectives  81 us (16%)
  starting transfers between devices  33.6 us (6%)
  matrix products  19.1 us (4%)
  between operations  14.1 us (3%)
  other arithmetic  12 us (2%)
  local copies, waits for them, and re-layouts  5.72 us (1%)
    all_gather x2, waiting for transfers between devices, sent_together(): filled = lax.all_gather(both, axis, axis=dim, tiled=True)  252 us
    all_gather x1, waiting for transfers between devices, gathered_by_axis(): filled = lax.all_gather(filled, axes[number], axis=dim, tiled=True)  68 us
    all_gather x3, blocking collectives, gathered_by_axis(): filled = lax.all_gather(filled, axes[number], axis=dim, tiled=True)  52.5 us
    all_to_all x1, blocking collectives, sent_and_summed(): tiles = lax.all_to_all(in_blocks(shard, dim, size), axis, 0, 0, tiled=True)  28.6 us
    all_to_all x2, starting transfers between devices, copy_for_each(): lax.all_to_all(jnp.broadcast_to(shard[None], (size, *shard.shape)), axis,...  19.4 us
    all_gather x2, waiting for transfers between devices, gather_turned(): filled, at, outs = (lax.all_gather(both, axis, axis=0, tiled=True), 0, [])  15 us
    all_to_all x1, starting transfers between devices, body(): lax.all_to_all(head_rows, 'tp', split_axis=1, concat_axis=0, tiled=True)  14.1 us
    all_to_all x2, waiting for transfers between devices, copy_for_each(): lax.all_to_all(jnp.broadcast_to(shard[None], (size, *shard.shape)), axis,...  14 us
  transfers between devices with their start and end apart: 8, of which 6 were waited for; matrix products, arithmetic and copies ran while one was open for 5% of the time, Pallas kernels for 0%

commit v1 on v0

--- a/solution.py
+++ b/solution.py
@@ -149,6 +149,12 @@
     ff_down,
     final_gain,
 ):
+
+    def _group_waves(patch):
+        return jnp.concatenate(
+            lax.all_to_all(jnp.stack(jnp.split(patch, lax.psum(1, "tp"), axis=1)), "tp", 0, 0), 0
+        )
+
     rows = tokens.shape[0]
     heads_here = head_rates.shape[0]
     groups = lax.axis_size("tp")
@@ -170,7 +176,7 @@
     gated = (normret * jax.nn.silu(gproj)).astype(jnp.bfloat16)
     all_heads = gather_directly(gated, "tp", 1)
     head_rows = gathered_by_axis(out_weight, FS, 1)
-    feature_block = lax.all_to_all(head_rows, "tp", split_axis=1, concat_axis=0, tiled=True)
+    feature_block = _group_waves(head_rows)
     width = all_heads.shape[1] // groups
     left = all_heads.reshape(rows, groups, width)
     right = feature_block.reshape(groups, width, feature_block.shape[1])

time: 517 us -> 517 us (level)
  no operation moved by 1% of the time
where the time goes in v1:
time: 517 us; the launch traced here: 516 us
  waiting for transfers between devices  345 us (67%)
  blocking collectives  81 us (16%)
  starting transfers between devices  33.6 us (6%)
  matrix products  19.1 us (4%)
  between operations  14.1 us (3%)
  other arithmetic  12 us (2%)
  local copies, waits for them, and re-layouts  9.81 us (2%)
    all_gather x2, waiting for transfers between devices, sent_together(): filled = lax.all_gather(both, axis, axis=dim, tiled=True)  248 us
    all_gather x1, waiting for transfers between devices, gathered_by_axis(): filled = lax.all_gather(filled, axes[number], axis=dim, tiled=True)  68 us
    all_gather x3, blocking collectives, gathered_by_axis(): filled = lax.all_gather(filled, axes[number], axis=dim, tiled=True)  52.5 us
    all_to_all x1, blocking collectives, sent_and_summed(): tiles = lax.all_to_all(in_blocks(shard, dim, size), axis, 0, 0, tiled=True)  28.6 us
    all_to_all x2, starting transfers between devices, copy_for_each(): lax.all_to_all(jnp.broadcast_to(shard[None], (size, *shard.shape)), axis,...  19.4 us
    all_gather x2, waiting for transfers between devices, gather_turned(): filled, at, outs = (lax.all_gather(both, axis, axis=0, tiled=True), 0, [])  15 us
    all_to_all x1, starting transfers between devices, _group_waves(): lax.all_to_all(jnp.stack(jnp.split(patch, lax.psum(1, 'tp'), axis=1)), 't...  14.1 us
    all_to_all x2, waiting for transfers between devices, copy_for_each(): lax.all_to_all(jnp.broadcast_to(shard[None], (size, *shard.shape)), axis,...  14 us
  transfers between devices with their start and end apart: 8, of which 6 were waited for; matrix products, arithmetic and copies ran while one was open for 5% of the time, Pallas kernels for 0%

profile of v1, /device:TPU:1, one launch (start us, length us, event | category | flops | bytes accessed | tf_op | source)
XLA Modules:
  0.0 515.8 jit_solution(14410864325760942766)
XLA Ops:
  6.5 0.7 reshape.395
  7.2 1.6 pad_maximum_fusion
  8.8 0.0 all-gather.8.cloned.1.call-start
  8.9 1.4 pad_maximum_fusion.3
  10.3 0.0 all-gather.8.cloned.1.call-update
  10.3 10.6 %all_gather.26 = bf16[128,128]{0,1:T(8,128)(2,1)S(1)} all-gather(bf16[128,32]{0,1:T(8,128)(2,1)} %param.22), channel_id=1, replica_groups=mesh['fs_0'=16,'fs_1'=4,'tp'=8] {'fs_1'}, dimensions={1}, use_global_device_ids=true | all-gather | bytes 40960 | tf_op jit(solution)/shard_map/all_gather | solution.py:55
  20.9 0.1 copy.26
  21.0 31.9 %all_gather.27 = bf16[128,2048]{1,0:T(8,128)(2,1)S(1)} all-gather(bf16[128,128]{1,0:T(8,128)(2,1)S(1)} %copy.26), channel_id=1, replica_groups=mesh['fs_0'=16,'fs_1'=4,'tp'=8] {'fs_0'}, dimensions={1}, use_global_device_ids=true | all-gather | bytes 557056 | tf_op jit(solution)/shard_map/all_gather | solution.py:55
  52.9 0.6 fusion.44
  53.6 0.6 fusion.43
  54.2 0.6 fusion.42
  54.8 0.6 fusion.41
  55.4 0.6 fusion.40
  56.1 0.6 fusion.39
  56.7 0.6 fusion.38
  57.3 0.6 fusion.37
  58.0 14.1 %all-to-all-start.1 = ((bf16[8,128,256]{2,1,0:T(8,128)(2,1)}), bf16[8,128,256]{2,1,0:T(8,128)(2,1)S(1)}, u32[]{:S(2)}, u32[]{:S(2)}) async-start(bf16[8,128,256]{2,1,0:T(8,128)(2,1)} %fusion.37), calls=%async_computation.1 | async-start | bytes 1048576 | tf_op jit(solution)/shard_map/all_to_all | solution.py:155
  72.9 0.1 multiply_exponential_fusion
  73.0 1.6 fusion.4
  74.6 0.8 slice_convert_fusion.1
  75.4 105.0 %all-gather.8.cloned.1.call-done = bf16[2048,384]{1,0:T(8,128)(2,1)} async-done(((bf16[32,384]{1,0:T(8,128)(2,1)}), bf16[2048,384]{1,0:T(8,128)(2,1)}) %all-gather.8.cloned.1.call-update) | async-done | bytes 1572880 | tf_op jit(solution)/shard_map/all_gather | solution.py:31
  180.3 2.0 convolution_bitcast_fusion
  182.4 1.6 convolution_bitcast_fusion.1
  184.0 0.2 fusion.65
  184.3 0.2 convolution_multiply_fusion
  184.6 1.5 convolution_convert_fusion.2
  186.1 0.2 fusion.81
  186.3 0.2 convolution_bitcast_fusion.2
  186.5 5.0 while.13
  186.5 0.6 dynamic_slice.22
  187.8 0.6 constant_dynamic-slice_fusion.2
  188.4 0.7 bitcast_add_fusion.2
  189.0 0.6 dynamic_slice.22
  190.3 0.6 constant_dynamic-slice_fusion.2
  190.9 0.7 bitcast_add_fusion.2
  191.6 0.5 multiply_reduce_fusion.1
  192.0 0.1 broadcast_multiply_fusion
  192.2 1.6 fusion.34
  193.8 0.9 broadcast_in_dim.29
  194.6 15.1 %all-to-all-start = ((bf16[8,256,128]{2,1,0:T(8,128)(2,1)}), bf16[8,256,128]{2,1,0:T(8,128)(2,1)S(1)}, u32[]{:S(2)}, u32[]{:S(2)}) async-start(bf16[8,256,128]{2,1,0:T(8,128)(2,1)} %broadcast_in_dim.29), calls=%async_computation | async-start | bytes 1048576 | tf_op jit(solution)/shard_map/all_to_all | solution.py:43
  209.7 9.3 %all-to-all-done = bf16[8,256,128]{2,1,0:T(8,128)(2,1)S(1)} async-done(((bf16[8,256,128]{2,1,0:T(8,128)(2,1)}), bf16[8,256,128]{2,1,0:T(8,128)(2,1)S(1)}, u32[]{:S(2)}, u32[]{:S(2)}) %all-to-all-start) | async-done | bytes 524320 | tf_op jit(solution)/shard_map/all_to_all | solution.py:43
  219.1 0.4 convert_reduce_fusion.1
  219.6 0.7 pad_maximum_fusion.1
  220.2 0.0 all-gather.10.cloned.1.call-update
  220.2 0.0 all-gather.12.cloned.1.call-start
  220.3 0.7 pad_maximum_fusion.2
  221.1 0.0 all-gather.14.cloned.1.call-start
  221.1 10.0 %all_gather.30 = bf16[704,128]{0,1:T(8,128)(2,1)} all-gather(bf16[704,32]{0,1:T(8,128)(2,1)S(1)} %copy-done.5), channel_id=1, replica_groups=mesh['fs_0'=16,'fs_1'=4,'tp'=8] {'fs_1'}, dimensions={1}, use_global_device_ids=true | all-gather | bytes 225280 | tf_op jit(solution)/shard_map/all_gather | solution.py:55
  231.1 0.0 all-gather.14.cloned.1.call-update
  231.1 15.0 %all-gather.10.cloned.1.call-done = bf16[2048,257]{0,1:T(8,128)(2,1)} async-done(((bf16[256,257]{0,1:T(8,128)(2,1)}), bf16[2048,257]{0,1:T(8,128)(2,1)}) %all-gather.10.cloned.1.call-update) | async-done | bytes 1052688 | tf_op jit(solution)/shard_map/all_gather | solution.py:20
  246.1 1.5 fusion.7
  247.6 0.8 slice_convert_fusion
  248.4 142.7 %all-gather.12.cloned.1.call-done = bf16[2048,1408]{1,0:T(8,128)(2,1)} async-done(((bf16[32,1408]{1,0:T(8,128)(2,1)}), bf16[2048,1408]{1,0:T(8,128)(2,1)}) %all-gather.12.cloned.1.call-update) | async-done | bytes 5767184 | tf_op jit(solution)/shard_map/all_gather | solution.py:31
  391.1 3.7 fusion.2
  394.7 68.0 %all-gather.14.cloned.1.call-done = bf16[704,2048]{0,1:T(8,128)(2,1)} async-done(((bf16[704,128]{0,1:T(8,128)(2,1)}), bf16[704,2048]{0,1:T(8,128)(2,1)}) %all-gather.14.cloned.1.call-update) | async-done | bytes 2883600 | tf_op jit(solution)/shard_map/all_gather | solution.py:55
  462.8 7.2 %convolution_convert_fusion = bf16[256,2048]{1,0:T(8,128)(2,1)S(1)} fusion(bf16[704,2048]{0,1:T(8,128)(2,1)} %all-gather.14.cloned.1.call-done, bf16[2048,1408]{1,0:T(8,128)(2,1)} %all-gather.12.cloned.1.call-done, f32[256,704]{0,1:T(8,128)S(1)} %fusion.2, f32[2048]{0:T(1024)S(1)} %bitcast.110, f32[256]{0:T(256)S(1)} %add_rsqrt_fusion.1, ...), kind=kOutput, calls=%fused_computation.12 | convolution fusion | flops 1480097792 | bytes 9118720 | tf_op jit(solution)/shard_map/dot_general | solution.py:194
  470.0 0.1 copy.32
  470.1 28.6 %all_to_all.20 = bf16[8,256,256]{2,1,0:T(8,128)(2,1)S(1)} all-to-all(bf16[8,256,256]{2,1,0:T(8,128)(2,1)S(1)} %bitcast.99), channel_id=1, replica_groups=mesh['fs_0'=16,'fs_1'=4,'tp'=8] {'tp'}, dimensions={0} | all-to-all | bytes 2097152 | tf_op jit(solution)/shard_map/all_to_all | solution.py:67
  498.7 0.1 convert_reduce_fusion
  498.8 0.1 multiply_reduce_fusion
  498.9 0.6 broadcast_in_dim.30
  499.5 4.3 all-to-all-start.3
  503.8 4.6 all-to-all-done.3
  508.5 0.8 multiply_convert_fusion
  (51 shorter events, 0.4 us)
Async XLA Ops:
  6.5 66.3 %copy-start.6 = (f32[2]{0:T(128)S(1)}, f32[2]{0:T(128)}, u32[]{:S(2)}) copy-start(f32[2]{0:T(128)} %param.24) | copy-start | bytes 28
  6.5 66.4 %all-gather.6.cloned.1.call-start = ((), (), s32[]{:S(2)}) async-start(), calls=%async_computation.4 | async-start | bytes 1216512 | tf_op jit(solution)/shard_map/all_gather | solution.py:20
  8.8 171.5 %all-gather.8.cloned.1.call-start = ((), (), s32[]{:S(2)}) async-start(), calls=%async_computation.5 | async-start | bytes 1597440 | tf_op jit(solution)/shard_map/all_gather | solution.py:31
  58.0 135.8 %all-to-all-start.1 = ((bf16[8,128,256]{2,1,0:T(8,128)(2,1)}), bf16[8,128,256]{2,1,0:T(8,128)(2,1)S(1)}, u32[]{:S(2)}, u32[]{:S(2)}) async-start(bf16[8,128,256]{2,1,0:T(8,128)(2,1)} %fusion.37), calls=%async_computation.1 | async-start | bytes 1048576 | tf_op jit(solution)/shard_map/all_to_all | solution.py:155
  73.0 109.4 %copy-start = (bf16[2048,257]{0,1:T(8,128)(2,1)S(1)}, bf16[2048,257]{0,1:T(8,128)(2,1)}, u32[]{:S(2)}) copy-start(bf16[2048,257]{0,1:T(8,128)(2,1)} %all-gather.6.cloned.1.call-done) | copy-start | bytes 3158020
  192.2 17.6 %copy-start.7 = (bf16[256]{0:T(256)(128)(2,1)S(1)}, bf16[256]{0:T(256)(128)(2,1)}, u32[]{:S(2)}) copy-start(bf16[256]{0:T(256)(128)(2,1)} %param.25) | copy-start | bytes 1540
  193.7 25.8 %copy-start.2 = (bf16[256,256]{1,0:T(8,128)(2,1)S(1)}, bf16[256,256]{1,0:T(8,128)(2,1)}, u32[]{:S(2)}) copy-start(bf16[256,256]{1,0:T(8,128)(2,1)} %param.16) | copy-start | bytes 393220
  193.7 26.6 %copy-start.3 = (bf16[32,704]{1,0:T(8,128)(2,1)S(1)}, bf16[32,704]{1,0:T(8,128)(2,1)}, u32[]{:S(2)}) copy-start(bf16[32,704]{1,0:T(8,128)(2,1)} %param.27) | copy-start | bytes 135172
  193.8 26.6 %copy-start.4 = (bf16[32,704]{1,0:T(8,128)(2,1)S(1)}, bf16[32,704]{1,0:T(8,128)(2,1)}, u32[]{:S(2)}) copy-start(bf16[32,704]{1,0:T(8,128)(2,1)} %param.26) | copy-start | bytes 135172
  193.8 27.3 %copy-start.5 = (bf16[704,32]{0,1:T(8,128)(2,1)S(1)}, bf16[704,32]{0,1:T(8,128)(2,1)}, u32[]{:S(2)}) copy-start(bf16[704,32]{0,1:T(8,128)(2,1)} %param.28) | copy-start | bytes 135172
  194.6 24.4 %all-to-all-start = ((bf16[8,256,128]{2,1,0:T(8,128)(2,1)}), bf16[8,256,128]{2,1,0:T(8,128)(2,1)S(1)}, u32[]{:S(2)}, u32[]{:S(2)}) async-start(bf16[8,256,128]{2,1,0:T(8,128)(2,1)} %broadcast_in_dim.29), calls=%async_computation | async-start | bytes 1048576 | tf_op jit(solution)/shard_map/all_to_all | solution.py:43
  209.7 36.4 %all-gather.10.cloned.1.call-start = ((), (), s32[]{:S(2)}) async-start(), calls=%async_computation.6 | async-start | bytes 1216512 | tf_op jit(solution)/shard_map/all_gather | solution.py:20
  220.2 170.8 %all-gather.12.cloned.1.call-start = ((), (), s32[]{:S(2)}) async-start(), calls=%async_computation.7 | async-start | bytes 5857280 | tf_op jit(solution)/shard_map/all_gather | solution.py:31
  221.1 241.7 %all-gather.14.cloned.1.call-start = ((), (), s32[]{:S(2)}) async-start(), calls=%async_computation.8 | async-start | bytes 3342336 | tf_op jit(solution)/shard_map/all_gather | solution.py:55
  391.1 71.7 %copy-start.1 = (bf16[2048,257]{0,1:T(8,128)(2,1)S(1)}, bf16[2048,257]{0,1:T(8,128)(2,1)}, u32[]{:S(2)}) copy-start(bf16[2048,257]{0,1:T(8,128)(2,1)} %all-gather.10.cloned.1.call-done) | copy-start | bytes 3158020
  470.1 33.7 %copy-start.8 = (bf16[256]{0:T(256)(128)(2,1)S(1)}, bf16[256]{0:T(256)(128)(2,1)}, u32[]{:S(2)}) copy-start(bf16[256]{0:T(256)(128)(2,1)} %param.29) | copy-start | bytes 1540
  499.5 8.9 %all-to-all-start.3 = ((f32[8,256,1]{1,2,0:T(1,128)}), f32[8,256,1]{1,2,0:T(1,128)S(1)}, u32[]{:S(2)}, u32[]{:S(2)}) async-start(f32[8,256,1]{1,2,0:T(1,128)} %broadcast_in_dim.30), calls=%async_computation.3 | async-start | bytes 16384 | tf_op jit(solution)/shard_map/all_to_all | solution.py:43
Sparse Core Ops, SparseCore 0:
  9.4 36.6 all-gather.5
  49.1 131.1 all-gather.7
  220.4 25.6 all-gather.9
  248.9 142.1 all-gather.11
  393.0 69.7 all-gather.13
